TPU v7x, 32 devices: a whole 2x2x4 slice. The times are simulated.
32 devices in a mesh: sp: 16 (over z, y, x), tp: 2 (over core).
Axes of the slice: x: 2, y: 2, z: 4, core: 2. Of those that a mesh axis runs over, the one named last changes fastest.
Arguments:
- resid: bfloat16 [3072, 2048], P('sp'), may hold values from -6 to 6
- query: bfloat16 [3072, 2048], P('sp', 'tp'), may hold values from -6 to 6
- key: bfloat16 [3072, 1024], P('sp', 'tp'), may hold values from -6 to 6
- value: bfloat16 [3072, 1024], P('sp', 'tp'), may hold values from -6 to 6
- q_gain: float32 [128], replicated, may hold values from 0.3 to 5, as said below
- k_gain: float32 [128], replicated, may hold values from 0.3 to 5, as said below
- out_weight: bfloat16 [2048, 2048], P('tp'), may hold values from -0.125 to 0.125
- norm_gain: float32 [2048], replicated, may hold values from 0.1 to 1.9
- gate_weight: bfloat16 [2048, 5632], P('sp', 'tp'), may hold values from -0.125 to 0.125
- up_weight: bfloat16 [2048, 5632], P('sp', 'tp'), may hold values from -0.125 to 0.125
- down_weight: bfloat16 [5632, 2048], P('tp', 'sp'), may hold values from -0.078125 to 0.078125
Outputs:
- mixed: bfloat16 [3072, 2048], P(('sp', 'tp'))
Inputs may be any that keep to these rules, and one draw needn't show every extreme that they name: `q_gain`: positive gains. `k_gain`: positive gains.
All inputs are finite; a program needn't handle non-finite values.
Results may differ from a plain program's by a relative error of at most 0.012.
The roundings to bfloat16 on the way count: a program that leaves them out, or rounds other values in their place, can miss the bound.
Values may be sent and summed in bfloat16 or wider, within the bound.
A program may use at most 128 MiB of HBM per device.

v0:
```python
import jax
import jax.numpy as jnp
from jax import lax
from jax.sharding import PartitionSpec as P

GRID_W = 64


EPSILON = 1e-06


def rotate(values, positions):
    dim_size = values.shape[-1]
    half_dim = dim_size // 2
    quarter = half_dim // 2
    inverse = 10000.0 ** (-jnp.arange(quarter, dtype=jnp.float32) / quarter)
    outputs = []
    for axis_pos, coords in enumerate((positions // GRID_W, positions % GRID_W)):
        angles = coords.astype(jnp.float32)[:, None] * inverse[None, :]
        cosine = jnp.cos(angles)[:, None, :]
        sine = jnp.sin(angles)[:, None, :]
        section = values[..., axis_pos * half_dim : (axis_pos + 1) * half_dim]
        first_half = section[..., :quarter]
        second_half = section[..., quarter:]
        outputs += [
            first_half * cosine - second_half * sine,
            second_half * cosine + first_half * sine,
        ]
    return jnp.concatenate(outputs, axis=-1)


def prepare(projected, gain, positions):
    values = projected.astype(jnp.float32)
    normed = values * lax.rsqrt(jnp.mean(values * values, axis=-1, keepdims=True) + EPSILON) * gain
    return rotate(normed, positions).astype(jnp.bfloat16)


def normalize(stream, gain):
    values = stream.astype(jnp.float32)
    return (
        values * lax.rsqrt(jnp.mean(values * values, axis=-1, keepdims=True) + EPSILON) * gain
    ).astype(jnp.bfloat16)


def body(
    resid,
    query,
    key,
    value,
    q_gain,
    k_gain,
    out_weight,
    norm_gain,
    gate_weight,
    up_weight,
    down_weight,
):
    rows_here = query.shape[0]
    head_dim = q_gain.shape[0]
    heads_here = query.shape[1] // head_dim
    kv_here = key.shape[1] // head_dim
    group_size = heads_here // kv_here
    score_scale = head_dim ** (-0.5)
    positions = lax.axis_index("sp") * rows_here + jnp.arange(rows_here, dtype=jnp.int32)
    q_rot = prepare(query.reshape(rows_here, heads_here, head_dim), q_gain, positions)
    k_rot = prepare(key.reshape(rows_here, kv_here, head_dim), k_gain, positions)
    val_rows = value.reshape(rows_here, kv_here, head_dim)
    grouped = q_rot.reshape(rows_here, kv_here, group_size, head_dim)

    def key_block(carry, block):
        maxima, totals, accum = carry
        block_keys, block_vals = block
        scores = (
            jnp.einsum("qkgd,skd->kgqs", grouped, block_keys, preferred_element_type=jnp.float32)
            * score_scale
        )
        new_max = jnp.maximum(maxima, jnp.max(scores, axis=-1))
        shrink = jnp.exp(maxima - new_max)
        weights = jnp.exp(scores - new_max[..., None])
        totals = totals * shrink + jnp.sum(weights, axis=-1)
        accum = accum * shrink[..., None] + jnp.einsum(
            "kgqs,skd->kgqd",
            weights.astype(jnp.bfloat16),
            block_vals,
            preferred_element_type=jnp.float32,
        )
        return ((new_max, totals, accum), None)

    start_max = jnp.full((kv_here, group_size, rows_here), -1e30, jnp.float32)
    start_total = jnp.zeros((kv_here, group_size, rows_here), jnp.float32)
    start_accum = jnp.zeros((kv_here, group_size, rows_here, head_dim), jnp.float32)
    carry = (start_max, start_total, start_accum)
    key_part = lax.all_gather(k_rot, "sp", axis=0, tiled=True)
    val_part = lax.all_gather(val_rows, "sp", axis=0, tiled=True)
    length = key_part.shape[0]
    factor = 4
    span = rows_here * factor
    turns = length // span
    key_blocks = key_part.reshape(turns, span, kv_here, head_dim)
    val_blocks = val_part.reshape(turns, span, kv_here, head_dim)
    carry, _ = lax.scan(key_block, carry, (key_blocks, val_blocks))
    maxima, totals, accum = carry
    attn = (
        jnp.transpose(accum / totals[..., None], (2, 0, 1, 3))
        .reshape(rows_here, heads_here * head_dim)
        .astype(jnp.bfloat16)
    )
    share = rows_here // lax.axis_size("tp")
    my_first = lax.axis_index("tp") * share
    proj = lax.psum_scatter(
        jnp.dot(attn, out_weight, preferred_element_type=jnp.float32).astype(jnp.bfloat16),
        "tp",
        scatter_dimension=0,
        tiled=True,
    ).astype(jnp.float32)
    my_resid = lax.dynamic_slice_in_dim(resid, my_first, share, 0)
    my_stream = (my_resid.astype(jnp.float32) + proj).astype(jnp.bfloat16)
    mixer_rows = lax.all_gather(normalize(my_stream, norm_gain), "tp", axis=0, tiled=True)

    def add_rows(shard_rows):
        return jnp.dot(mixer_rows, shard_rows, preferred_element_type=jnp.float32)

    gate = add_rows(lax.all_gather(gate_weight, "sp", axis=0, tiled=True))
    up_part = add_rows(lax.all_gather(up_weight, "sp", axis=0, tiled=True))
    hidden = (jax.nn.silu(gate) * up_part).astype(jnp.bfloat16)
    down_whole = lax.all_gather(down_weight, "sp", axis=1, tiled=True)
    down = lax.psum_scatter(
        jnp.dot(hidden, down_whole, preferred_element_type=jnp.float32).astype(jnp.bfloat16),
        "tp",
        scatter_dimension=0,
        tiled=True,
    ).astype(jnp.float32)
    return (my_stream.astype(jnp.float32) + 0.5 * down).astype(jnp.bfloat16)


def solution(mesh):
    placed = (
        P("sp", None),
        P("sp", "tp"),
        P("sp", "tp"),
        P("sp", "tp"),
        P(),
        P(),
        P("tp", None),
        P(),
        P("sp", "tp"),
        P("sp", "tp"),
        P("tp", "sp"),
    )
    return jax.shard_map(
        body, mesh=mesh, in_specs=placed, out_specs=P(("sp", "tp"), None), check_vma=False
    )
```

profile of v0, /device:TPU:0, one launch (start us, length us, event | category | flops | bytes accessed | tf_op | source)
XLA Modules:
  0.0 702.4 jit_solution(25329568361684075)
XLA Ops:
  6.6 1.1 reshape.193
  7.7 0.3 multiply_reduce_fusion.1
  8.0 0.9 multiply_multiply_fusion.1
  8.9 0.8 multiply_cosine_fusion.1
  9.7 0.7 subtract_convert_fusion.3
  10.4 1.3 pad_maximum_fusion.1
  11.8 0.7 reshape.191
  12.9 0.3 multiply_reduce_fusion
  13.4 0.3 multiply_multiply_fusion
  13.6 0.7 subtract_convert_fusion.1
  14.6 0.5 pad_maximum_fusion
  15.1 67.4 %all-gather.6.cloned.1.call-done = bf16[3072,4,128]{2,1,0:T(4,128)(2,1)} async-done(((bf16[192,4,128]{2,1,0:T(4,128)(2,1)}), bf16[3072,4,128]{2,1,0:T(4,128)(2,1)}) %all-gather.6.cloned.1.call-update) | async-done | bytes 3145744 | tf_op jit(solution)/shard_map/all_gather | solution.py:93
  82.5 69.2 %all-gather.8.cloned.1.call-done = bf16[3072,4,128]{2,1,0:T(4,128)(2,1)} async-done(((bf16[192,4,128]{2,1,0:T(4,128)(2,1)}), bf16[3072,4,128]{2,1,0:T(4,128)(2,1)}) %all-gather.8.cloned.1.call-update) | async-done | bytes 3145744 | tf_op jit(solution)/shard_map/all_gather | solution.py:94
  151.7 40.1 %while.15 = (s32[]{:T(128)}, f32[4,2,192]{2,1,0:T(2,128)S(1)}, f32[4,2,192]{2,1,0:T(2,128)S(1)}, f32[4,2,192,128]{3,2,1,0:T(8,128)S(1)}, bf16[4,768,4,128]{3,2,1...) while((s32[]{:T(128)}, f32[4,2,192]{2,1,0:T(2,128)S(1)}, ...), condition=%wide.region_5.6_spmd.clone, body=%wide.region_2.5_spmd.clone.sunk | while | flops 614014464 | bytes 39813256 | solution.py:101
  151.7 1.9 constant_dynamic-slice_fusion.3
  153.6 2.9 bitcast_reduce_fusion.2
  156.5 3.5 fusion.42
  160.3 1.4 fusion.44
  161.7 1.9 constant_dynamic-slice_fusion.3
  163.6 2.9 bitcast_reduce_fusion.2
  166.6 3.5 fusion.42
  170.3 1.4 fusion.44
  171.7 1.9 constant_dynamic-slice_fusion.3
  173.6 2.9 bitcast_reduce_fusion.2
  176.6 3.5 fusion.42
  180.3 1.4 fusion.44
  181.7 1.9 constant_dynamic-slice_fusion.3
  183.7 2.9 bitcast_reduce_fusion.2
  186.6 3.5 fusion.42
  190.2 0.2 copy-done
  190.3 1.4 fusion.44
  191.8 0.3 fusion.19
  192.0 0.4 copy.56
  192.5 0.3 convert_element_type.83
  192.8 4.1 convolution_convert_fusion.1
  196.9 0.5 all-gather.10.cloned.1.call-update
  197.5 0.5 all-gather.12.cloned.1.call-update
  198.1 0.5 all-gather.14.cloned.1.call-update
  198.7 5.1 reduce-scatter.3.cloned.1.call-done
  203.8 1.2 fusion.15
  205.2 2.5 all_gather.20
  207.7 141.2 %all-gather.10.cloned.1.call-done = bf16[2048,2816]{1,0:T(8,128)(2,1)} async-done(((bf16[128,2816]{1,0:T(8,128)(2,1)}), bf16[2048,2816]{1,0:T(8,128)(2,1)}) %all-gather.10.cloned.1.call-update) | async-done | bytes 11534352 | tf_op jit(solution)/shard_map/all_gather | solution.py:123
  348.9 6.7 fusion.24
  355.6 135.6 %all-gather.12.cloned.1.call-done = bf16[2048,2816]{1,0:T(8,128)(2,1)} async-done(((bf16[128,2816]{1,0:T(8,128)(2,1)}), bf16[2048,2816]{1,0:T(8,128)(2,1)}) %all-gather.12.cloned.1.call-update) | async-done | bytes 11534352 | tf_op jit(solution)/shard_map/all_gather | solution.py:124
  491.2 182.8 %all-gather.14.cloned.1.call-done = bf16[2816,2048]{1,0:T(8,128)(2,1)} async-done(((bf16[2816,128]{1,0:T(8,128)(2,1)}), bf16[2816,2048]{1,0:T(8,128)(2,1)}) %all-gather.14.cloned.1.call-update) | async-done | bytes 11534352 | tf_op jit(solution)/shard_map/all_gather | solution.py:126
  674.0 13.2 %convolution_convert_fusion = bf16[192,2048]{1,0:T(8,128)(2,1)} fusion(bf16[2816,2048]{1,0:T(8,128)(2,1)} %all-gather.14.cloned.1.call-done, bf16[192,2048]{1,0:T(8,128)(2,1)S(1)} %all_gather.20, bf16[2048,2816]{1,0:T(8,128)(2,1)} %all-gather.12.cloned.1.call-done, f32[192,2816]{1,0:T(8,128)S(1)} %fusion.24), kind=kOutput, calls=%fused_computation.23 | convolution fusion | flops 4432822272 | bytes 26804224 | tf_op jit(solution)/shard_map/dot_general | solution.py:128
  687.2 6.5 reduce-scatter.5.cloned.1.call-done
  693.7 1.9 fusion.18
  (57 shorter events, 1.8 us)
Async XLA Ops:
  6.5 5.2 copy-start.2
  6.5 6.1 copy-start.1
  6.5 75.9 %all-gather.6.cloned.1.call-start = ((), (), s32[]{:S(2)}) async-start(), calls=%async_computation.2 | async-start | bytes 3342336 | tf_op jit(solution)/shard_map/all_gather | solution.py:93
  8.0 5.3 copy-start.5
  11.7 140.0 %all-gather.8.cloned.1.call-start = ((), (), s32[]{:S(2)}) async-start(), calls=%async_computation.3 | async-start | bytes 3342336 | tf_op jit(solution)/shard_map/all_gather | solution.py:94
  12.5 191.2 %reduce-scatter.3.cloned.1.call-start = ((), (), s32[]{:S(2)}) async-start(), calls=%async_computation.4 | async-start | bytes 1179648 | tf_op jit(solution)/shard_map/reduce_scatter | solution.py:110
  156.5 3.8 copy-start
  166.5 3.8 copy-start
  176.6 3.8 copy-start
  186.6 3.8 copy-start
  192.5 11.3 %copy-start.3 = (bf16[192,2048]{1,0:T(8,128)(2,1)S(1)}, bf16[192,2048]{1,0:T(8,128)(2,1)}, u32[]{:S(2)}) copy-start(bf16[192,2048]{1,0:T(8,128)(2,1)} %param.13) | copy-start | bytes 2359300
  192.7 12.3 %copy-start.4 = (f32[2048]{0:T(1024)S(1)}, f32[2048]{0:T(1024)}, u32[]{:S(2)}) copy-start(f32[2048]{0:T(1024)} %param.20) | copy-start | bytes 24580
  196.9 152.0 %all-gather.10.cloned.1.call-start = ((), (), s32[]{:S(2)}) async-start(), calls=%async_computation.5 | async-start | bytes 12255232 | tf_op jit(solution)/shard_map/all_gather | solution.py:123
  197.5 293.7 %all-gather.12.cloned.1.call-start = ((), (), s32[]{:S(2)}) async-start(), calls=%async_computation.6 | async-start | bytes 12255232 | tf_op jit(solution)/shard_map/all_gather | solution.py:124
  198.1 475.9 %all-gather.14.cloned.1.call-start = ((), (), s32[]{:S(2)}) async-start(), calls=%async_computation.7 | async-start | bytes 12255232 | tf_op jit(solution)/shard_map/all_gather | solution.py:126
  198.6 495.1 %reduce-scatter.5.cloned.1.call-start = ((), (), s32[]{:S(2)}) async-start(), calls=%async_computation.8 | async-start | bytes 1179648 | tf_op jit(solution)/shard_map/reduce_scatter | solution.py:127
Sparse Core Ops, SparseCore 0:
  11.9 70.5 all-gather.5
  85.2 66.3 all-gather.7
  197.0 6.6 reduce-scatter.2
  206.4 142.5 all-gather.9
  351.5 139.5 all-gather.11
  493.7 180.2 all-gather.13
  687.3 6.3 reduce-scatter.4
where the time goes:
time: 703 us; the launch traced here: 702 us
  waiting for transfers between devices  609 us (87%)
  matrix products  41.2 us (6%)
  other arithmetic  23.7 us (3%)
  between operations  13.8 us (2%)
  local copies, waits for them, and re-layouts  11.4 us (2%)
    all_gather x1, waiting for transfers between devices, body(): down_whole = lax.all_gather(down_weight, 'sp', axis=1, tiled=True)  183 us
    all_gather x1, waiting for transfers between devices, body(): gate = add_rows(lax.all_gather(gate_weight, 'sp', axis=0, tiled=True))  141 us
    all_gather x1, waiting for transfers between devices, body(): up_part = add_rows(lax.all_gather(up_weight, 'sp', axis=0, tiled=True))  136 us
    all_gather x1, waiting for transfers between devices, body(): val_part = lax.all_gather(val_rows, 'sp', axis=0, tiled=True)  69.2 us
    all_gather x1, waiting for transfers between devices, body(): key_part = lax.all_gather(k_rot, 'sp', axis=0, tiled=True)  67.4 us
    reduce_sum x4, other arithmetic, key_block(): totals = totals * shrink + jnp.sum(weights, axis=-1)  14.2 us
  transfers between devices with their start and end apart: 7, of which 7 were waited for; matrix products, arithmetic and copies ran while one was open for 2% of the time, Pallas kernels for 0%

commit v1 on v0

--- a/solution.py
+++ b/solution.py
@@ -42,7 +42,7 @@
     ).astype(jnp.bfloat16)
 
 
-def body(
+def whole_body(
     resid,
     query,
     key,
@@ -133,6 +133,111 @@
     return (my_stream.astype(jnp.float32) + 0.5 * down).astype(jnp.bfloat16)
 
 
+SPLIT = 4
+
+
+def fits(n_sp, kv_here, hidden_here):
+    return n_sp % SPLIT == 0 and kv_here % SPLIT == 0 and hidden_here % (64 * SPLIT) == 0
+
+
+def groups_of(n_sp):
+    ranks = n_sp // SPLIT
+    tokens = [[part * ranks + rank for part in range(SPLIT)] for rank in range(ranks)]
+    hidden = [[part * ranks + rank for rank in range(ranks)] for part in range(SPLIT)]
+    return tokens, hidden
+
+
+def body(
+    resid,
+    query,
+    key,
+    value,
+    q_gain,
+    k_gain,
+    out_weight,
+    norm_gain,
+    gate_weight,
+    up_weight,
+    down_weight,
+):
+    rows = query.shape[0]
+    head_dim = q_gain.shape[0]
+    heads_here = query.shape[1] // head_dim
+    kv_here = key.shape[1] // head_dim
+    n_sp = lax.axis_size("sp")
+    if not fits(n_sp, kv_here, gate_weight.shape[1]):
+        return whole_body(
+            resid, query, key, value, q_gain, k_gain, out_weight, norm_gain, gate_weight, up_weight, down_weight
+        )
+    tok_groups, hid_groups = groups_of(n_sp)
+    ranks = n_sp // SPLIT
+    group_size = heads_here // kv_here
+    kv_part = kv_here // SPLIT
+
+    def swap(array):
+        return lax.all_to_all(array, "sp", 0, 0, axis_index_groups=tok_groups, tiled=True)
+
+    def spread(array, axis):
+        return lax.all_gather(array, "sp", axis=axis, axis_index_groups=hid_groups, tiled=True)
+
+    positions = lax.axis_index("sp") * rows + jnp.arange(rows, dtype=jnp.int32)
+    q_rot = prepare(query.reshape(rows, heads_here, head_dim), q_gain, positions)
+    k_rot = prepare(key.reshape(rows, kv_here, head_dim), k_gain, positions)
+    cut = lambda a: a.reshape(a.shape[0], SPLIT, -1).transpose(1, 0, 2).reshape(SPLIT * a.shape[0], -1)
+    k_rot, val = cut(k_rot), cut(value)
+    pair = swap(jnp.concatenate([k_rot, val], axis=1))
+    pair = spread(pair, 0)
+    q_mine = swap(cut(q_rot))
+    width = kv_part * head_dim
+    keys = pair[:, :width].reshape(-1, kv_part, head_dim)
+    vals = pair[:, width:].reshape(-1, kv_part, head_dim)
+    grouped = q_mine.reshape(SPLIT * rows, kv_part, group_size, head_dim)
+    gate_up = spread(swap(jnp.concatenate([cut(gate_weight), cut(up_weight)], axis=1)), 0)
+    depth = gate_weight.shape[0]
+    gate_up = gate_up.reshape(ranks, SPLIT, depth, -1).transpose(1, 0, 2, 3).reshape(n_sp * depth, -1)
+    down_w = swap(down_weight)
+    part = down_weight.shape[0] // SPLIT
+    down_w = down_w.reshape(SPLIT, part, -1)
+    down_w = lax.all_gather(down_w, "sp", axis=1, axis_index_groups=hid_groups)
+    down_w = jnp.transpose(down_w, (2, 0, 1, 3)).reshape(part, -1)
+    scores = jnp.einsum("qkgd,skd->kgqs", grouped, keys, preferred_element_type=jnp.float32) * head_dim ** (-0.5)
+    weights = jnp.exp(scores - jnp.max(scores, axis=-1, keepdims=True))
+    totals = jnp.sum(weights, axis=-1)
+    accum = jnp.einsum("kgqs,skd->kgqd", weights.astype(jnp.bfloat16), vals, preferred_element_type=jnp.float32)
+    attn = jnp.transpose(accum / totals[..., None], (2, 0, 1, 3)).astype(jnp.bfloat16).reshape(SPLIT * rows, -1)
+    attn = swap(attn).reshape(SPLIT, rows, -1).transpose(1, 0, 2).reshape(rows, -1)
+    return finish(attn, resid, out_weight, norm_gain, gate_up, down_w, tok_groups)
+
+
+def finish(attn, resid, out_weight, norm_gain, gate_up, down_w, tok_groups):
+    rows = resid.shape[0]
+    n_tp = lax.axis_size("tp")
+    share = rows // n_tp
+    my_first = lax.axis_index("tp") * share
+    proj = lax.psum_scatter(
+        jnp.dot(attn, out_weight, preferred_element_type=jnp.float32).astype(jnp.bfloat16),
+        "tp",
+        scatter_dimension=0,
+        tiled=True,
+    ).astype(jnp.float32)
+    my_resid = lax.dynamic_slice_in_dim(resid, my_first, share, 0)
+    my_stream = (my_resid.astype(jnp.float32) + proj).astype(jnp.bfloat16)
+    normed = normalize(my_stream, norm_gain)
+    normed = lax.all_gather(normed, "sp", axis=0, axis_index_groups=tok_groups, tiled=False)
+    normed = lax.all_gather(normed, "tp", axis=0, tiled=False)
+    normed = normed.reshape(n_tp * SPLIT * share, -1)
+    both = jnp.dot(normed, gate_up, preferred_element_type=jnp.float32)
+    gate, up_part = jnp.split(both, 2, axis=1)
+    hidden = (jax.nn.silu(gate) * up_part).astype(jnp.bfloat16)
+    down = jnp.dot(hidden, down_w, preferred_element_type=jnp.float32).astype(jnp.bfloat16)
+    down = lax.psum_scatter(down, "tp", scatter_dimension=0, tiled=True)
+    down = lax.all_to_all(
+        down.reshape(SPLIT, share, -1), "sp", 0, 0, axis_index_groups=tok_groups, tiled=True
+    )
+    down = jnp.sum(down.astype(jnp.float32), axis=0)
+    return (my_stream.astype(jnp.float32) + 0.5 * down).astype(jnp.bfloat16)
+
+
 def solution(mesh):
     placed = (
         P("sp", None),

time: 703 us -> 376 us (0.53)
  waiting for transfers between devices: 609 us -> 119 us
  blocking collectives: 2.55 us -> 169 us
  local copies, waits for them, and re-layouts: 11.4 us -> 19 us
    all_gather x5, waiting for transfers between devices: 596 us -> 99.1 us  [the longest x2 73.6 us: spread(): lax.all_gather(array, 'sp', axis=axis, axis_index_groups=hid_groups, tile...]
    all_to_all x0 -> x6, blocking collectives: none -> 169 us  [the longest x5 127 us: swap(): lax.all_to_all(array, 'sp', 0, 0, axis_index_groups=tok_groups, tiled=True)]
    reshape x1 -> x4, local copies, waits for them, and re-layouts: 0.73 us -> 10.2 us  [the longest x1 5.84 us: body(): gate_up.reshape(ranks, SPLIT, depth, -1).transpose(1, 0, 2, 3)]
    dynamic_slice x4 -> x0, local copies, waits for them, and re-layouts: 7.66 us -> none  [body(): carry, _ = lax.scan(key_block, carry, (key_blocks, val_blocks))]
    reduce_scatter x2, waiting for transfers between devices: 11.6 us -> 18.9 us  [the longest x1 12.5 us: finish(): down = lax.psum_scatter(down, 'tp', scatter_dimension=0, tiled=True)]
    dot_general x11 -> x5, matrix products: 41.2 us -> 35.7 us  [the longest x1 9.63 us: body(): jnp.einsum('kgqs,skd->kgqd', weights.astype(jnp.bfloat16), vals, preferre...]
    reduce_sum x4 -> x2, other arithmetic: 14.2 us -> 9.81 us  [the longest x1 9.54 us: body(): totals = jnp.sum(weights, axis=-1)]
  transfers between devices with their start and end apart: 7 -> 7, of which waited for: 7 -> 6; matrix products, arithmetic and copies ran while one was open for 2% -> 5% of each run, Pallas kernels for 0% -> 0%
where the time goes in v1:
time: 376 us; the launch traced here: 375 us
  blocking collectives  169 us (45%)
  waiting for transfers between devices  119 us (32%)
  matrix products  35.7 us (9%)
  local copies, waits for them, and re-layouts  19 us (5%)
  other arithmetic  18.3 us (5%)
  between operations  13.8 us (4%)
    all_to_all x5, blocking collectives, swap(): lax.all_to_all(array, 'sp', 0, 0, axis_index_groups=tok_groups, tiled=True)  127 us
    all_gather x2, waiting for transfers between devices, spread(): lax.all_gather(array, 'sp', axis=axis, axis_index_groups=hid_groups, tile...  73.6 us
    all_to_all x1, blocking collectives, finish(): lax.all_to_all(down.reshape(SPLIT, share, -1), 'sp', 0, 0, axis_index_gro...  42.3 us
    all_gather x1, waiting for transfers between devices, body(): down_w = lax.all_gather(down_w, 'sp', axis=1, axis_index_groups=hid_groups)  17.8 us
    reduce_scatter x1, waiting for transfers between devices, finish(): down = lax.psum_scatter(down, 'tp', scatter_dimension=0, tiled=True)  12.5 us
    dot_general x1, matrix products, body(): jnp.einsum('kgqs,skd->kgqd', weights.astype(jnp.bfloat16), vals, preferre...  9.63 us
    reduce_sum x1, other arithmetic, body(): totals = jnp.sum(weights, axis=-1)  9.54 us
    dot_general x1, matrix products, body(): jnp.einsum('qkgd,skd->kgqs', grouped, keys, preferred_element_type=jnp.fl...  9.18 us
  transfers between devices with their start and end apart: 7, of which 6 were waited for; matrix products, arithmetic and copies ran while one was open for 5% of the time, Pallas kernels for 0%

profile of v1, /device:TPU:0, one launch (start us, length us, event | category | flops | bytes accessed | tf_op | source)
XLA Modules:
  0.0 374.9 jit_solution(12952029491829130340)
XLA Ops:
  6.6 1.1 reshape.268
  7.6 0.3 multiply_reduce_fusion.1
  7.9 1.0 reshape.257
  8.9 0.9 multiply_multiply_fusion.1
  9.8 0.8 multiply_cosine_fusion.1
  10.6 0.7 subtract_convert_fusion.3
  11.3 0.6 maximum_bitcast_fusion
  12.0 0.2 pad_maximum_fusion.1
  12.2 17.9 %all_to_all.47 = bf16[4,192,256]{2,1,0:T(8,128)(2,1)} all-to-all(bf16[4,192,256]{2,1,0:T(8,128)(2,1)S(1)} %copy.87), channel_id=1, replica_groups={{0,8,16,24},{2,10,18,26},{4,12,20,28},{6,14,22,30},{1,9,17,25},{3,11,19..., dimensions={0} | all-to-all | bytes 786432 | tf_op jit(solution)/shard_map/all_to_all | solution.py:178
  30.3 0.1 copy.102
  30.5 0.3 multiply_reduce_fusion
  30.8 0.1 copy.89
  31.0 0.3 multiply_multiply_fusion
  31.2 0.7 subtract_convert_fusion.1
  32.0 0.5 pad_maximum_fusion.2
  32.5 0.3 convert_element_type.84
  32.8 13.8 %all_to_all.48 = bf16[4,192,256]{2,1,0:T(8,128)(2,1)S(1)} all-to-all(bf16[4,192,256]{2,1,0:T(8,128)(2,1)S(1)} %copy.90), channel_id=1, replica_groups={{0,8,16,24},{2,10,18,26},{4,12,20,28},{6,14,22,30},{1,9,17,25},{3,11,19..., dimensions={0} | all-to-all | bytes 786432 | tf_op jit(solution)/shard_map/all_to_all | solution.py:178
  46.7 13.6 %all-gather.9.cloned.1.call-done = bf16[3072,256]{1,0:T(8,128)(2,1)} async-done(((bf16[768,256]{1,0:T(8,128)(2,1)}), bf16[3072,256]{1,0:T(8,128)(2,1)}) %all-gather.9.cloned.1.call-update) | async-done | bytes 1572880 | tf_op jit(solution)/shard_map/all_gather | solution.py:181
  60.3 9.2 %bitcast_reduce_fusion = (f32[2,768]{1,0:T(2,128)S(1)}, f32[3072,768,2]{1,0,2:T(8,128)}) fusion(bf16[768,2,128]{2,1,0:T(2,128)(2,1)S(1)} %reshape.258, bf16[3072,256]{1,0:T(8,128)(2,1)} %all-gather.9.cloned.1.call-done), kind=kOutput, calls=%fused_computation.1 | convolution fusion | flops 1217395200 | bytes 20060160 | tf_op jit(solution)/shard_map/qkgd,skd->kgqs/dot_general | solution.py:203
  69.5 9.5 %fusion.1 = f32[2,768]{1,0:T(2,128)S(1)} fusion(f32[3072,768,2]{1,0,2:T(8,128)} %get-tuple-element.26, f32[2,768]{1,0:T(2,128)S(1)} %get-tuple-element.25), kind=kLoop, calls=%fused_computation.3 | loop fusion | flops 14154240 | bytes 18886656 | tf_op jit(solution)/shard_map/reduce_sum | solution.py:205
  79.0 9.6 %fusion.15 = bf16[768,1,2,128]{3,0,2,1:T(8,128)(2,1)S(1)} fusion(f32[3072,768,2]{1,0,2:T(8,128)} %get-tuple-element.26, f32[2,768]{1,0:T(2,128)S(1)} %get-tuple-element.25, bf16[3072,256]{1,0:T(8,128)(2,1)S(1)} %copy-done.4, f32[2,768]{1,0:T(2,128)S(1)} %fusion.1), kind=kOutput, calls=%fused_computation.19 | convolution fusion | flops 1222508544 | bytes 20066304 | tf_op jit(solution)/shard_map/kgqs,skd->kgqd/dot_general | solution.py:206
  88.7 0.4 copy.93
  89.1 0.3 all_to_all.34
  89.3 15.9 %all_to_all.49 = bf16[4,192,256]{2,1,0:T(8,128)(2,1)S(1)} all-to-all(bf16[4,192,256]{2,1,0:T(8,128)(2,1)S(1)} %all_to_all.34), channel_id=1, replica_groups={{0,8,16,24},{2,10,18,26},{4,12,20,28},{6,14,22,30},{1,9,17,25},{3,11,19..., dimensions={0} | all-to-all | bytes 786432 | tf_op jit(solution)/shard_map/all_to_all | solution.py:178
  105.3 4.2 %convolution_convert_fusion.1 = bf16[192,2048]{1,0:T(8,128)(2,1)} fusion(bf16[192,1024]{1,0:T(8,128)(2,1)S(1)} %bitcast.90, bf16[1024,2048]{1,0:T(8,128)(2,1)} %param.17), kind=kOutput, calls=%fused_computation.9 | convolution fusion | flops 805699584 | bytes 5373952 | tf_op jit(solution)/shard_map/dot_general | solution.py:218
  109.6 6.4 %reduce-scatter.3.cloned.1.call-done = bf16[96,2048]{1,0:T(8,128)(2,1)} async-done(((bf16[192,2048]{1,0:T(8,128)(2,1)}), bf16[96,2048]{1,0:T(8,128)(2,1)}) %reduce-scatter.3.cloned.1.call-update) | async-done | bytes 393232 | tf_op jit(solution)/shard_map/reduce_scatter | solution.py:217
  116.0 1.2 fusion.18
  117.3 0.9 fusion.20
  118.2 40.3 %all_to_all.50 = bf16[4,704,128]{2,1,0:T(8,128)(2,1)} all-to-all(bf16[4,704,128]{2,1,0:T(8,128)(2,1)S(1)} %bitcast.92), channel_id=1, replica_groups={{0,8,16,24},{2,10,18,26},{4,12,20,28},{6,14,22,30},{1,9,17,25},{3,11,19..., dimensions={0} | all-to-all | bytes 1441792 | tf_op jit(solution)/shard_map/all_to_all | solution.py:178
  158.6 0.3 copy.95
  159.0 0.3 copy.96
  159.3 0.1 pad_maximum_fusion
  159.4 38.8 %all_to_all.51 = bf16[4,128,1408]{1,2,0:T(8,128)(2,1)S(1)} all-to-all(bf16[4,128,1408]{1,2,0:T(8,128)(2,1)S(1)} %pad_maximum_fusion), channel_id=1, replica_groups={{0,8,16,24},{2,10,18,26},{4,12,20,28},{6,14,22,30},{1,9,17,25},{3,11,19..., dimensions={0} | all-to-all | bytes 2883584 | tf_op jit(solution)/shard_map/all_to_all | solution.py:178
  198.3 1.6 copy.97
  199.9 0.5 all-gather.15.cloned.1.call-update
  200.4 0.3 reduce-scatter.5.cloned.1.call-start
  200.7 17.8 %all-gather.17.cloned.1.call-done = bf16[4,2816,128]{2,1,0:T(8,128)(2,1)} async-done(((bf16[4,704,128]{2,1,0:T(8,128)(2,1)}), bf16[4,2816,128]{2,1,0:T(8,128)(2,1)}) %all-gather.17.cloned.1.call-update) | async-done | bytes 2883600 | tf_op jit(solution)/shard_map/all_gather | solution.py:201
  218.5 4.0 %copy.99 = bf16[704,4,4,128]{3,2,1,0:T(4,128)(2,1)S(1)} copy(bf16[704,4,4,128]{3,0,2,1:T(8,128)(2,1)} %bitcast.82) | data formatting | bytes 5767168 | tf_op jit(solution)/shard_map/transpose | solution.py:202
  222.5 3.4 reshape.266
  225.9 60.0 %all-gather.11.cloned.1.call-done = bf16[2048,1408]{1,0:T(8,128)(2,1)} async-done(((bf16[512,1408]{1,0:T(8,128)(2,1)}), bf16[2048,1408]{1,0:T(8,128)(2,1)}) %all-gather.11.cloned.1.call-update) | async-done | bytes 5767184 | tf_op jit(solution)/shard_map/all_gather | solution.py:181
  285.9 5.8 %copy.98 = bf16[4,4,128,1408]{3,2,0,1:T(8,128)(2,1)} copy(bf16[4,4,128,1408]{3,2,1,0:T(8,128)(2,1)} %bitcast.79) | data formatting | bytes 11534336 | tf_op jit(solution)/shard_map/reshape | solution.py:197
  291.7 7.7 %all-gather.15.cloned.1.call-done = bf16[8,96,2048]{2,1,0:T(8,128)(2,1)} async-done(((bf16[4,96,2048]{2,1,0:T(8,128)(2,1)}), bf16[8,96,2048]{2,1,0:T(8,128)(2,1)}) %all-gather.15.cloned.1.call-update) | async-done | bytes 3145744 | tf_op jit(solution)/shard_map/all_gather | solution.py:227
  299.4 8.5 %fusion.29 = f32[768,1408]{1,0:T(8,128)S(1)} fusion(bf16[768,2048]{1,0:T(8,128)(2,1)} %bitcast.93, bf16[2048,1408]{1,0:T(8,128)(2,1)} %bitcast.80), kind=kOutput, calls=%fused_computation.65 | convolution fusion | flops 4429185024 | bytes 13238272 | tf_op jit(solution)/shard_map/dot_general | solution.py:229
  308.0 4.2 %convolution_convert_fusion = bf16[768,2048]{1,0:T(8,128)(2,1)} fusion(bf16[704,2048]{1,0:T(8,128)(2,1)S(1)} %copy-done, f32[768,1408]{1,0:T(8,128)S(1)} %fusion.29), kind=kOutput, calls=%fused_computation.7 | convolution fusion | flops 2219409408 | bytes 10747904 | tf_op jit(solution)/shard_map/dot_general | solution.py:232
  312.2 12.5 %reduce-scatter.5.cloned.1.call-done = bf16[384,2048]{1,0:T(8,128)(2,1)} async-done(((bf16[768,2048]{1,0:T(8,128)(2,1)}), bf16[384,2048]{1,0:T(8,128)(2,1)}) %reduce-scatter.5.cloned.1.call-update) | async-done | bytes 1572880 | tf_op jit(solution)/shard_map/reduce_scatter | solution.py:233
  324.7 42.3 %all_to_all.52 = bf16[4,96,2048]{2,1,0:T(8,128)(2,1)S(1)} all-to-all(bf16[4,96,2048]{2,1,0:T(8,128)(2,1)} %bitcast.86), channel_id=1, replica_groups={{0,8,16,24},{2,10,18,26},{4,12,20,28},{6,14,22,30},{1,9,17,25},{3,11,19..., dimensions={0} | all-to-all | bytes 3145728 | tf_op jit(solution)/shard_map/all_to_all | solution.py:234
  367.0 0.3 convert_reduce_fusion
  367.2 0.9 fusion.21
  (42 shorter events, 0.8 us)
Async XLA Ops:
  6.5 53.8 %all-gather.9.cloned.1.call-start = ((), (), s32[]{:S(2)}) async-start(), calls=%async_computation.8 | async-start | bytes 1966080 | tf_op jit(solution)/shard_map/all_gather | solution.py:181
  10.6 19.6 %copy-start.5 = (bf16[192,1024]{1,0:T(8,128)(2,1)S(1)}, bf16[192,1024]{1,0:T(8,128)(2,1)}, u32[]{:S(2)}) copy-start(bf16[192,1024]{1,0:T(8,128)(2,1)} %param.12) | copy-start | bytes 1179652
  12.0 19.0 %copy-start.8 = (f32[128]{0:T(128)S(1)}, f32[128]{0:T(128)}, u32[]{:S(2)}) copy-start(f32[128]{0:T(128)} %param.15) | copy-start | bytes 1540
  30.2 85.8 %reduce-scatter.3.cloned.1.call-start = ((), (), s32[]{:S(2)}) async-start(), calls=%async_computation.9 | async-start | bytes 1179648 | tf_op jit(solution)/shard_map/reduce_scatter | solution.py:217
  69.5 9.5 %copy-start.4 = (bf16[3072,256]{1,0:T(8,128)(2,1)S(1)}, bf16[3072,256]{1,0:T(8,128)(2,1)}, u32[]{:S(2)}) copy-start(bf16[3072,256]{1,0:T(8,128)(2,1)} %all-gather.9.cloned.1.call-done) | copy-start | bytes 4718596
  105.3 10.7 %copy-start.6 = (bf16[192,2048]{1,0:T(8,128)(2,1)S(1)}, bf16[192,2048]{1,0:T(8,128)(2,1)}, u32[]{:S(2)}) copy-start(bf16[192,2048]{1,0:T(8,128)(2,1)} %param.11) | copy-start | bytes 2359300
  105.3 11.9 %copy-start.7 = (f32[2048]{0:T(1024)S(1)}, f32[2048]{0:T(1024)}, u32[]{:S(2)}) copy-start(f32[2048]{0:T(1024)} %param.18) | copy-start | bytes 24580
  105.3 12.9 %copy-start.1 = (bf16[2816,128]{1,0:T(8,128)(2,1)S(1)}, bf16[2816,128]{1,0:T(8,128)(2,1)}, u32[]{:S(2)}) copy-start(bf16[2816,128]{1,0:T(8,128)(2,1)} %param.21) | copy-start | bytes 2162692
  109.5 49.1 %copy-start.2 = (bf16[128,2816]{1,0:T(8,128)(2,1)S(1)}, bf16[128,2816]{1,0:T(8,128)(2,1)}, u32[]{:S(2)}) copy-start(bf16[128,2816]{1,0:T(8,128)(2,1)} %param.19) | copy-start | bytes 2162692
  109.5 49.4 %copy-start.3 = (bf16[128,2816]{1,0:T(8,128)(2,1)S(1)}, bf16[128,2816]{1,0:T(8,128)(2,1)}, u32[]{:S(2)}) copy-start(bf16[128,2816]{1,0:T(8,128)(2,1)} %param.20) | copy-start | bytes 2162692
  109.6 90.3 %all-gather.13.cloned.1.call-start = ((), (), s32[]{:S(2)}) async-start(), calls=%async_computation.12 | async-start | bytes 1966080 | tf_op jit(solution)/shard_map/all_gather | solution.py:226
  118.2 100.3 %all-gather.17.cloned.1.call-start = ((), (), s32[]{:S(2)}) async-start(), calls=%async_computation.14 | async-start | bytes 3604480 | tf_op jit(solution)/shard_map/all_gather | solution.py:201
  158.6 127.3 %all-gather.11.cloned.1.call-start = ((), (), s32[]{:S(2)}) async-start(), calls=%async_computation.10 | async-start | bytes 7208960 | tf_op jit(solution)/shard_map/all_gather | solution.py:181
  199.8 99.6 %all-gather.15.cloned.1.call-start = ((), (), s32[]{:S(2)}) async-start(), calls=%async_computation.13 | async-start | bytes 4718592 | tf_op jit(solution)/shard_map/all_gather | solution.py:227
  200.4 124.3 %reduce-scatter.5.cloned.1.call-start = ((), (), s32[]{:S(2)}) async-start(), calls=%async_computation.11 | async-start | bytes 4718592 | tf_op jit(solution)/shard_map/reduce_scatter | solution.py:233
  299.4 8.5 %copy-start = (bf16[704,2048]{1,0:T(8,128)(2,1)S(1)}, bf16[704,2048]{1,0:T(8,128)(2,1)}, u32[]{:S(2)}) copy-start(bf16[704,2048]{1,0:T(8,128)(2,1)} %reshape.266) | copy-start | bytes 8650756
Sparse Core Ops, SparseCore 0:
  30.3 29.9 all-gather.8
  109.7 6.2 reduce-scatter.2
  118.3 58.6 all-gather.12
  178.7 39.7 all-gather.16
  220.2 65.6 all-gather.10
  287.3 12.1 all-gather.14
  312.3 12.3 reduce-scatter.4

commit v2 on v1

--- a/solution.py
+++ b/solution.py
@@ -1,6 +1,11 @@
+import functools
+import math
+
 import jax
 import jax.numpy as jnp
 from jax import lax
+from jax.experimental import pallas as pl
+from jax.experimental.pallas import tpu as pltpu
 from jax.sharding import PartitionSpec as P
 
 GRID_W = 64
@@ -147,6 +152,309 @@
     return tokens, hidden
 
 
+MESH = pl.DeviceIdType.MESH
+
+
+def layer_kernel(
+    ranks,
+    head_dim,
+    kv_ref,
+    q_ref,
+    gu_ref,
+    dn_ref,
+    ow_ref,
+    resid_ref,
+    gain_ref,
+    out_ref,
+    kvb,
+    qb,
+    asend,
+    ab,
+    wgu,
+    wdn,
+    pj,
+    prv,
+    nb,
+    st,
+    dsb,
+    drv,
+    ds2,
+    dzb,
+    local_sem,
+    kvz_s, kvz_r, kvx_s, kvx_r, q_s, q_r, gz_s, gz_r, dz_s, dz_r,
+    gx_s, gx_r, dx_s, dx_r, gh_s, gh_r, dh_s, dh_r,
+    at_s, at_r, pj_s, pj_r, nz_s, nz_r, np_s, np_r, dp_s, dp_r, fz_s, fz_r,
+):
+    sp = lax.axis_index("sp")
+    core = lax.axis_index("tp")
+    part = sp // ranks
+    rank = sp % ranks
+    rows = q_ref.shape[1]
+    share = rows // 2
+    depth = gu_ref.shape[1]
+    width = dn_ref.shape[1]
+    cols = dn_ref.shape[2]
+    group = q_ref.shape[2] // head_dim
+    other = 1 - core
+    flips = (1, 2, 3)
+
+    def flip(e):
+        x = rank % 2
+        y = rank // 2
+        nx = 1 - x if e % 2 else x
+        ny = 1 - y if e // 2 else y
+        return ny * 2 + nx
+
+    def peer_part(dz):
+        return ((part + dz) % SPLIT) * ranks + rank
+
+    def from_part(dz):
+        return (part + SPLIT - dz) % SPLIT
+
+    def near(e):
+        return part * ranks + flip(e)
+
+    sent = []
+
+    def send(src, dst, s_sem, r_sem, target):
+        copy = pltpu.make_async_remote_copy(
+            src_ref=src, dst_ref=dst, send_sem=s_sem, recv_sem=r_sem, device_id=target, device_id_type=MESH
+        )
+        copy.start()
+        sent.append(copy)
+
+    def landed(dst, s_sem, r_sem):
+        pltpu.make_async_remote_copy(
+            src_ref=dst, dst_ref=dst, send_sem=s_sem, recv_sem=r_sem, device_id=(sp, other), device_id_type=MESH
+        ).wait_recv()
+
+    def gu_at(source, first=0, count=None):
+        return wgu.at[pl.ds(pl.multiple_of(source * depth + first, 16), depth if count is None else count)]
+
+    def dn_at(source, first=0, count=None):
+        return wdn.at[pl.ds(first, width if count is None else count), pl.ds(pl.multiple_of(source * cols, cols), cols)]
+
+    locals_ = [
+        pltpu.make_async_copy(kv_ref.at[part], kvb.at[part, rank], local_sem.at[0]),
+        pltpu.make_async_copy(q_ref.at[part], qb.at[part], local_sem.at[1]),
+        pltpu.make_async_copy(gu_ref.at[part], gu_at(sp), local_sem.at[2]),
+        pltpu.make_async_copy(dn_ref.at[part], dn_at(sp), local_sem.at[3]),
+    ]
+    for copy in locals_:
+        copy.start()
+    pad = wdn.shape[0] - width
+    wdn[pl.ds(width, pad), :] = jnp.zeros((pad, wdn.shape[1]), wdn.dtype)
+
+    barrier = pltpu.get_barrier_semaphore()
+    for dz in range(1, SPLIT):
+        pl.semaphore_signal(barrier, inc=1, device_id=(peer_part(dz), core), device_id_type=MESH)
+    for e in flips:
+        pl.semaphore_signal(barrier, inc=1, device_id=(near(e), core), device_id_type=MESH)
+    pl.semaphore_signal(barrier, inc=1, device_id=(sp, other), device_id_type=MESH)
+    pl.semaphore_wait(barrier, SPLIT - 1 + 3 + 1)
+
+    def to_part(dz):
+        return (part + dz) % SPLIT
+
+    for dz in range(1, SPLIT):
+        send(kv_ref.at[to_part(dz)], kvb.at[part, rank], kvz_s.at[dz], kvz_r.at[dz], (peer_part(dz), core))
+    for e in flips:
+        send(kv_ref.at[part], kvb.at[part, rank], kvx_s.at[0, e], kvx_r.at[0, e], (near(e), core))
+    for dz in range(1, SPLIT):
+        send(q_ref.at[to_part(dz)], qb.at[part], q_s.at[dz], q_r.at[dz], (peer_part(dz), core))
+    for e in (1, 2):
+        send(dn_ref.at[part], dn_at(sp), dx_s.at[0, e], dx_r.at[0, e], (near(e), core))
+    for dz in range(1, SPLIT):
+        send(gu_ref.at[to_part(dz)], gu_at(sp), gz_s.at[dz], gz_r.at[dz], (peer_part(dz), core))
+        send(dn_ref.at[to_part(dz)], dn_at(sp), dz_s.at[dz], dz_r.at[dz], (peer_part(dz), core))
+    for dz in range(1, SPLIT):
+        slot = kvb.at[from_part(dz), rank]
+        landed(slot, kvz_s.at[dz], kvz_r.at[dz])
+        for e in flips:
+            send(slot, slot, kvx_s.at[dz, e], kvx_r.at[dz, e], (near(e), core))
+    for e in (1, 2):
+        send(gu_ref.at[part], gu_at(sp), gx_s.at[0, e], gx_r.at[0, e], (near(e), core))
+
+    def pass_on(dz):
+        source = from_part(dz) * ranks + rank
+        landed(gu_at(source), gz_s.at[dz], gz_r.at[dz])
+        for e in (1, 2):
+            send(gu_at(source), gu_at(source), gx_s.at[dz, e], gx_r.at[dz, e], (near(e), core))
+        landed(dn_at(source), dz_s.at[dz], dz_r.at[dz])
+        for e in (1, 2):
+            send(dn_at(source), dn_at(source), dx_s.at[dz, e], dx_r.at[dz, e], (near(e), core))
+
+    def halves(dz):
+        for e in (1, 2):
+            source = from_part(dz) * ranks + flip(e)
+            across = (near(3 - e), core)
+            landed(gu_at(source), gx_s.at[dz, e], gx_r.at[dz, e])
+            half = gu_at(source, (e - 1) * depth // 2, depth // 2)
+            send(half, half, gh_s.at[dz, e], gh_r.at[dz, e], across)
+            landed(dn_at(source), dx_s.at[dz, e], dx_r.at[dz, e])
+            half = dn_at(source, (e - 1) * width // 2, width // 2)
+            send(half, half, dh_s.at[dz, e], dh_r.at[dz, e], across)
+
+    for dz in range(SPLIT):
+        for e in flips:
+            landed(kvb.at[from_part(dz), flip(e)], kvx_s.at[dz, e], kvx_r.at[dz, e])
+    locals_[0].wait()
+    locals_[1].wait()
+    for dz in range(1, SPLIT):
+        landed(qb.at[from_part(dz)], q_s.at[dz], q_r.at[dz])
+
+    factor = head_dim ** (-0.5) * math.log2(math.e)
+    length = SPLIT * ranks * rows
+
+    def attend(source, target):
+        @pl.loop(0, group)
+        def _(head):
+            lanes = pl.ds(pl.multiple_of(head * head_dim, head_dim), head_dim)
+            q = qb[source, :, lanes]
+            keys = kvb[:, :, :, pl.ds(0, head_dim)].reshape(length, head_dim)
+            scores = lax.dot_general(q, keys, (((1,), (1,)), ((), ())), preferred_element_type=jnp.float32)
+            peak = jnp.max(scores, axis=-1, keepdims=True)
+            weights = jnp.exp2((scores - peak) * factor)
+            total = jnp.sum(weights, axis=-1, keepdims=True)
+            vals = kvb[:, :, :, pl.ds(head_dim, head_dim)].reshape(length, head_dim)
+            summed = jnp.dot(weights.astype(jnp.bfloat16), vals, preferred_element_type=jnp.float32)
+            target[:, lanes] = (summed / total).astype(jnp.bfloat16)
+
+    for dz in (1, 2, 3):
+        attend(to_part(dz), asend.at[dz])
+        send(asend.at[dz], ab.at[part], at_s.at[dz], at_r.at[dz], (peer_part(dz), core))
+        if dz == 2:
+            pass_on(1)
+    attend(part, ab.at[part])
+    halves(0)
+    for dz in range(1, SPLIT):
+        landed(ab.at[from_part(dz)], at_s.at[dz], at_r.at[dz])
+
+    attn = jnp.concatenate([ab[index] for index in range(SPLIT)], axis=1)
+    tile = 512
+    for first in range(0, ow_ref.shape[1], tile):
+        block = jnp.dot(attn, ow_ref[:, first : first + tile], preferred_element_type=jnp.float32)
+        pj[:, :, first : first + tile] = block.astype(jnp.bfloat16).reshape(2, share, tile)
+    send(pj.at[other], prv, pj_s, pj_r, (sp, other))
+    pass_on(2)
+    landed(prv, pj_s, pj_r)
+    proj = pj[core].astype(jnp.float32) + prv[...].astype(jnp.float32)
+    stream = (resid_ref[...].astype(jnp.float32) + proj).astype(jnp.bfloat16)
+    st[...] = stream
+    wide = stream.astype(jnp.float32)
+    level = lax.rsqrt(jnp.mean(wide * wide, axis=-1, keepdims=True) + EPSILON)
+    nb[part, core] = (wide * level * gain_ref[...]).astype(jnp.bfloat16)
+    mine = nb.at[part, core]
+    for dz in range(1, SPLIT):
+        send(mine, mine, nz_s.at[dz], nz_r.at[dz], (peer_part(dz), core))
+    send(mine, mine, np_s.at[0], np_r.at[0], (sp, other))
+    halves(1)
+    pass_on(3)
+    halves(2)
+    for dz in range(1, SPLIT):
+        slot = nb.at[from_part(dz), core]
+        landed(slot, nz_s.at[dz], nz_r.at[dz])
+        send(slot, slot, np_s.at[dz], np_r.at[dz], (sp, other))
+    halves(3)
+    for dz in range(SPLIT):
+        for e in (1, 2):
+            source = from_part(dz) * ranks + flip(3)
+            landed(gu_at(source, (e - 1) * depth // 2, depth // 2), gh_s.at[dz, e], gh_r.at[dz, e])
+            landed(dn_at(source, (e - 1) * width // 2, width // 2), dh_s.at[dz, e], dh_r.at[dz, e])
+    locals_[2].wait()
+    locals_[3].wait()
+
+    main = width // 128 * 128
+    half_lane = width - main
+
+    def feed(source, partner_sem):
+        landed(nb.at[source, other], np_s.at[partner_sem], np_r.at[partner_sem])
+        x = nb[source].reshape(rows, nb.shape[-1])
+        pieces = []
+        gate = jnp.dot(x, wgu[:, pl.ds(0, main)], preferred_element_type=jnp.float32)
+        up = jnp.dot(x, wgu[:, pl.ds(main, main)], preferred_element_type=jnp.float32)
+        pieces.append((gate / (1.0 + jnp.exp(-gate)) * up).astype(jnp.bfloat16))
+        last = jnp.dot(x, wgu[:, pl.ds(2 * main, 128)], preferred_element_type=jnp.float32)
+        turned = pltpu.roll(last, half_lane, 1)
+        lane = lax.broadcasted_iota(jnp.int32, last.shape, 1)
+        tail = jnp.where(lane < half_lane, last / (1.0 + jnp.exp(-last)) * turned, 0.0)
+        pieces.append(tail.astype(jnp.bfloat16))
+        hidden = jnp.concatenate(pieces, axis=1)
+        for first in range(0, wdn.shape[1], tile):
+            block = jnp.dot(hidden, wdn[:, first : first + tile], preferred_element_type=jnp.float32)
+            dsb[source, :, :, first : first + tile] = block.astype(jnp.bfloat16).reshape(2, share, tile)
+
+    def pair_up(dz):
+        source = to_part(dz)
+        landed(drv.at[dz], dp_s.at[dz], dp_r.at[dz])
+        both = dsb[source, core].astype(jnp.float32) + drv[dz].astype(jnp.float32)
+        if dz == 0:
+            return both
+        ds2[dz] = both.astype(jnp.bfloat16)
+        send(ds2.at[dz], dzb.at[dz], fz_s.at[dz], fz_r.at[dz], (peer_part(dz), core))
+
+    order = (1, 2, 3, 0)
+    for place, dz in enumerate(order):
+        feed(to_part(dz), (SPLIT - dz) % SPLIT)
+        send(dsb.at[to_part(dz), other], drv.at[dz], dp_s.at[dz], dp_r.at[dz], (sp, other))
+        if place:
+            pair_up(order[place - 1])
+    down = pair_up(0)
+    for dz in range(1, SPLIT):
+        landed(dzb.at[dz], fz_s.at[dz], fz_r.at[dz])
+        down = down + dzb[dz].astype(jnp.float32)
+    out_ref[...] = (st[...].astype(jnp.float32) + 0.5 * down).astype(jnp.bfloat16)
+    for copy in sent:
+        copy.wait_send()
+
+
+def run_layer(kv, q, gate_up, down, out_weight, resid, gain, ranks, head_dim):
+    rows = q.shape[1]
+    share = rows // 2
+    model = resid.shape[1]
+    width = down.shape[1]
+    n_sp = ranks * SPLIT
+    half = jnp.bfloat16
+    dma = pltpu.SemaphoreType.DMA
+    per_part = [dma((SPLIT,))] * 2
+    per_near = [dma((SPLIT, 4))] * 2
+    anywhere = pl.BlockSpec(memory_space=pl.ANY)
+    inside = pl.BlockSpec(memory_space=pltpu.VMEM)
+    return pl.pallas_call(
+        functools.partial(layer_kernel, ranks, head_dim),
+        out_shape=jax.ShapeDtypeStruct((share, model), half),
+        in_specs=[anywhere] * 4 + [inside] * 3,
+        out_specs=inside,
+        scratch_shapes=[
+            pltpu.VMEM((SPLIT, ranks, rows, kv.shape[2]), half),
+            pltpu.VMEM(q.shape, half),
+            pltpu.VMEM(q.shape, half),
+            pltpu.VMEM(q.shape, half),
+            pltpu.VMEM((n_sp * gate_up.shape[1], gate_up.shape[2]), half),
+            pltpu.VMEM((-(-width // 128) * 128, model), half),
+            pltpu.VMEM((2, share, model), half),
+            pltpu.VMEM((share, model), half),
+            pltpu.VMEM((SPLIT, 2, share, model), half),
+            pltpu.VMEM((share, model), half),
+            pltpu.VMEM((SPLIT, 2, share, model), half),
+            pltpu.VMEM((SPLIT, share, model), half),
+            pltpu.VMEM((SPLIT, share, model), half),
+            pltpu.VMEM((SPLIT, share, model), half),
+            dma((4,)),
+        ]
+        + per_part + per_near + per_part * 3
+        + per_near * 4
+        + per_part + [dma, dma] + per_part * 4,
+        compiler_params=pltpu.CompilerParams(
+            collective_id=0, has_side_effects=True, vmem_limit_bytes=62 * 1024 * 1024
+        ),
+    )(kv, q, gate_up, down, out_weight, resid, gain)
+
+
+def in_kernel(n_sp, n_tp, kv_here, head_dim, width):
+    return n_sp == 4 * SPLIT and n_tp == 2 and kv_here == SPLIT and head_dim == 128 and width % 128 == 64
+
+
 def body(
     resid,
     query,
@@ -185,6 +493,27 @@
     k_rot = prepare(key.reshape(rows, kv_here, head_dim), k_gain, positions)
     cut = lambda a: a.reshape(a.shape[0], SPLIT, -1).transpose(1, 0, 2).reshape(SPLIT * a.shape[0], -1)
     k_rot, val = cut(k_rot), cut(value)
+    hidden_part = gate_weight.shape[1] // SPLIT
+    if in_kernel(n_sp, lax.axis_size("tp"), kv_here, head_dim, hidden_part):
+        stack = lambda a: a.reshape(SPLIT, a.shape[0] // SPLIT, -1)
+        main = hidden_part // 128 * 128
+        gate_cut, up_cut = stack(cut(gate_weight)), stack(cut(up_weight))
+        gate_up = jnp.concatenate(
+            [gate_cut[..., :main], up_cut[..., :main], gate_cut[..., main:], up_cut[..., main:]], axis=-1
+        )
+        share = rows // 2
+        my_resid = lax.dynamic_slice_in_dim(resid, lax.axis_index("tp") * share, share, 0)
+        return run_layer(
+            stack(jnp.concatenate([k_rot, val], axis=1)),
+            stack(cut(q_rot)),
+            gate_up,
+            stack(down_weight),
+            out_weight,
+            my_resid,
+            norm_gain[None, :],
+            ranks,
+            head_dim,
+        )
     pair = swap(jnp.concatenate([k_rot, val], axis=1))
     pair = spread(pair, 0)
     q_mine = swap(cut(q_rot))

time: 376 us -> 184 us (0.49)
  the two profiles are of different devices: /device:TPU:0 before, /device:TPU:26 now
where the time goes in v2:
time: 184 us
  Pallas kernels  165 us (90%)
  local copies, waits for them, and re-layouts  12.6 us (7%)
  other arithmetic  5.49 us (3%)
    pallas_call x1, Pallas kernels, run_layer(): pl.pallas_call(functools.partial(layer_kernel, ranks, head_dim), out_shap...  165 us
    unnamed x12, local copies, waits for them, and re-layouts  3.74 us

profile of v2, /device:TPU:26, one launch (start us, length us, event | category | flops | bytes accessed | tf_op | source)
XLA Modules:
  0.0 183.6 jit_solution(4997315651034161672)
XLA Ops:
  0.0 0.0 copy-start
  0.0 0.0 copy-start.2
  0.0 1.1 bitcast_bitcast_fusion
  1.1 1.1 reshape.184
  2.1 0.3 multiply_reduce_fusion.1
  2.4 0.1 copy.36
  2.5 1.1 fusion
  3.7 0.8 multiply_cosine_fusion.1
  4.4 0.0 copy-start.3
  4.4 0.4 subtract_convert_fusion.3
  4.8 0.3 maximum_bitcast_fusion
  5.1 0.8 pad_maximum_fusion.kv_ref
  5.9 0.0 copy-done.2
  5.9 0.1 convert_bitcast_fusion
  6.0 0.1 copy.48
  6.1 0.3 multiply_reduce_fusion
  6.4 0.1 copy.39
  6.5 0.1 copy.40
  6.6 0.0 copy-done.3
  6.6 0.3 multiply_multiply_fusion
  6.9 0.0 copy-start.1
  6.9 0.7 subtract_convert_fusion.1
  7.6 0.5 pad_maximum_fusion.1
  8.1 0.3 convert_element_type.40
  8.4 0.8 copy.52
  9.2 0.0 copy-done.1
  9.2 0.3 copy.42
  9.5 0.3 copy.43
  9.8 0.9 slice.68
  10.7 1.5 copy.44
  12.2 0.3 copy.45
  12.5 0.1 slice.69
  12.6 3.1 %concatenate.18.gu_ref = bf16[4,128,1408]{2,1,0:T(8,128)(2,1)} concatenate(bf16[4,128,640]{2,1,0:T(8,128)(2,1)} %slice.68, bf16[4,128,640]{2,1,0:T(8,128)(2,1)S(1)} %slice.69, bf16[4,128,64]{2,1,0:T(8,128)(2,1)S(1)} %slice.70, bf16[4,128,64]{2,1,0:T(8,128)(2,1)S(1)} %slice.71), dimensions={2} | concatenate | bytes 2883584 | tf_op jit(solution)/shard_map/concatenate | solution.py:501
  15.7 0.0 copy-done
  15.7 0.8 constant_dynamic-slice_fusion.resid_ref
  16.5 165.4 %shard_map.109 = bf16[96,2048]{1,0:T(8,128)(2,1)} custom-call(bf16[4,192,256]{2,1,0:T(8,128)(2,1)} %pad_maximum_fusion.kv_ref, bf16[4,192,256]{2,1,0:T(8,128)(2,1)} %bitcast.36, bf16[4,128,1408]{2,1,0:T(8,128)(2,1)} %concatenate.18.gu_ref, bf16[4,704,128]{2,1,0:T(8,128)(2,1)} %bitcast.37, bf16[1024,2048]{1,0:T(8,128)(2,1)} %ow_ref.1, ...), custom_call_target="tpu_custom_call" | custom-call | tf_op jit(solution)/shard_map/pallas_call | solution.py:423
  181.9 1.8 copy.54
  (6 shorter events, 0.1 us)
Async XLA Ops:
  0.0 15.7 %copy-start = (bf16[192,2048]{1,0:T(8,128)(2,1)S(1)}, bf16[192,2048]{1,0:T(8,128)(2,1)}, u32[]{:S(2)}) copy-start(bf16[192,2048]{1,0:T(8,128)(2,1)} %param.11) | copy-start | bytes 2359300
  0.0 5.9 %copy-start.2 = (bf16[192,1024]{1,0:T(8,128)(2,1)S(1)}, bf16[192,1024]{1,0:T(8,128)(2,1)}, u32[]{:S(2)}) copy-start(bf16[192,1024]{1,0:T(8,128)(2,1)} %param.12) | copy-start | bytes 1179652
  4.4 2.2 %copy-start.3 = (f32[128]{0:T(128)S(1)}, f32[128]{0:T(128)}, u32[]{:S(2)}) copy-start(f32[128]{0:T(128)} %param.15) | copy-start | bytes 1540
  6.9 2.3 %copy-start.1 = (bf16[128,2816]{1,0:T(8,128)(2,1)S(1)}, bf16[128,2816]{1,0:T(8,128)(2,1)}, u32[]{:S(2)}) copy-start(bf16[128,2816]{1,0:T(8,128)(2,1)} %param.19) | copy-start | bytes 2162692

commit v3 on v2

--- a/solution.py
+++ b/solution.py
@@ -180,6 +180,7 @@
     drv,
     ds2,
     dzb,
+    acc,
     local_sem,
     kvz_s, kvz_r, kvx_s, kvx_r, q_s, q_r, gz_s, gz_r, dz_s, dz_r,
     gx_s, gx_r, dx_s, dx_r, gh_s, gh_r, dh_s, dh_r,
@@ -216,12 +217,14 @@
 
     sent = []
 
-    def send(src, dst, s_sem, r_sem, target):
+    def send(src, dst, s_sem, r_sem, target, keep=True):
         copy = pltpu.make_async_remote_copy(
             src_ref=src, dst_ref=dst, send_sem=s_sem, recv_sem=r_sem, device_id=target, device_id_type=MESH
         )
         copy.start()
-        sent.append(copy)
+        if keep:
+            sent.append(copy)
+        return copy
 
     def landed(dst, s_sem, r_sem):
         pltpu.make_async_remote_copy(
@@ -344,18 +347,43 @@
     wide = stream.astype(jnp.float32)
     level = lax.rsqrt(jnp.mean(wide * wide, axis=-1, keepdims=True) + EPSILON)
     nb[part, core] = (wide * level * gain_ref[...]).astype(jnp.bfloat16)
+    ahead = [(part < SPLIT - 1, sp + ranks, -1), (part > 0, sp - ranks, 1)]
+
+    def step_on(source, step, way):
+        slot = nb.at[source, core]
+        go, target, _ = ahead[way]
+
+        @pl.when(go)
+        def _():
+            send(slot, slot, nz_s.at[way, step], nz_r.at[way, step], (target, core), keep=False)
+
+    def present(way, step):
+        source = part + ahead[way][2] * (step + 1)
+        return source, (source >= 0) & (source < SPLIT)
+
+    step_on(part, 0, 0)
+    step_on(part, 0, 1)
     mine = nb.at[part, core]
-    for dz in range(1, SPLIT):
-        send(mine, mine, nz_s.at[dz], nz_r.at[dz], (peer_part(dz), core))
-    send(mine, mine, np_s.at[0], np_r.at[0], (sp, other))
+    send(mine, mine, np_s.at[part], np_r.at[part], (sp, other))
+    def hop(step):
+        for way in (0, 1):
+            source, there = present(way, step)
+
+            @pl.when(there)
+            def _():
+                slot = nb.at[source, core]
+                landed(slot, nz_s.at[way, step], nz_r.at[way, step])
+                if step < SPLIT - 2:
+                    step_on(source, step + 1, way)
+                send(slot, slot, np_s.at[source], np_r.at[source], (sp, other), keep=False)
+
     halves(1)
     pass_on(3)
+    hop(0)
     halves(2)
-    for dz in range(1, SPLIT):
-        slot = nb.at[from_part(dz), core]
-        landed(slot, nz_s.at[dz], nz_r.at[dz])
-        send(slot, slot, np_s.at[dz], np_r.at[dz], (sp, other))
+    hop(1)
     halves(3)
+    hop(2)
     for dz in range(SPLIT):
         for e in (1, 2):
             source = from_part(dz) * ranks + flip(3)
@@ -367,8 +395,8 @@
     main = width // 128 * 128
     half_lane = width - main
 
-    def feed(source, partner_sem):
-        landed(nb.at[source, other], np_s.at[partner_sem], np_r.at[partner_sem])
+    def feed(source):
+        landed(nb.at[source, other], np_s.at[source], np_r.at[source])
         x = nb[source].reshape(rows, nb.shape[-1])
         pieces = []
         gate = jnp.dot(x, wgu[:, pl.ds(0, main)], preferred_element_type=jnp.float32)
@@ -384,28 +412,78 @@
             block = jnp.dot(hidden, wdn[:, first : first + tile], preferred_element_type=jnp.float32)
             dsb[source, :, :, first : first + tile] = block.astype(jnp.bfloat16).reshape(2, share, tile)
 
-    def pair_up(dz):
-        source = to_part(dz)
-        landed(drv.at[dz], dp_s.at[dz], dp_r.at[dz])
-        both = dsb[source, core].astype(jnp.float32) + drv[dz].astype(jnp.float32)
-        if dz == 0:
-            return both
-        ds2[dz] = both.astype(jnp.bfloat16)
-        send(ds2.at[dz], dzb.at[dz], fz_s.at[dz], fz_r.at[dz], (peer_part(dz), core))
-
-    order = (1, 2, 3, 0)
-    for place, dz in enumerate(order):
-        feed(to_part(dz), (SPLIT - dz) % SPLIT)
-        send(dsb.at[to_part(dz), other], drv.at[dz], dp_s.at[dz], dp_r.at[dz], (sp, other))
+    high, odd = part // 2, part % 2
+    order = (3 - 3 * high, 2 - 2 * odd + high, 1 + odd, part)
+    at_end = (part == 0) | (part == SPLIT - 1)
+    inner = (part > 0) & (part < SPLIT - 1)
+
+    def pair_sum(place):
+        landed(drv.at[place], dp_s.at[place], dp_r.at[place])
+        return dsb[order[place], core].astype(jnp.float32) + drv[place].astype(jnp.float32)
+
+    def onward(place, first):
+        target = order[place]
+        way = 1 - (target > part).astype(jnp.int32)
+        total = pair_sum(place)
+        if not first:
+            landed(dzb.at[way, target], fz_s.at[way, target], fz_r.at[way, target])
+            total = total + dzb[way, target].astype(jnp.float32)
+        ds2[target] = total.astype(jnp.bfloat16)
+        slot = dzb.at[way, target]
+        sender = fz_s.at[way, target]
+        send(ds2.at[target], slot, sender, fz_r.at[way, target], (sp + ranks * (1 - 2 * way), core), keep=False)
+
+    for place in range(SPLIT):
+        feed(order[place])
+        send(dsb.at[order[place], other], drv.at[place], dp_s.at[place], dp_r.at[place], (sp, other))
         if place:
-            pair_up(order[place - 1])
-    down = pair_up(0)
-    for dz in range(1, SPLIT):
-        landed(dzb.at[dz], fz_s.at[dz], fz_r.at[dz])
-        down = down + dzb[dz].astype(jnp.float32)
+
+            @pl.when(at_end)
+            def _():
+                onward(place - 1, True)
+
+    @pl.when(inner)
+    def _():
+        for place in range(SPLIT - 1):
+            onward(place, False)
+
+    acc[...] = pair_sum(SPLIT - 1)
+    for way, some in ((0, part > 0), (1, part < SPLIT - 1)):
+
+        @pl.when(some)
+        def _():
+            landed(dzb.at[way, part], fz_s.at[way, part], fz_r.at[way, part])
+            acc[...] += dzb[way, part].astype(jnp.float32)
+
+    down = acc[...]
     out_ref[...] = (st[...].astype(jnp.float32) + 0.5 * down).astype(jnp.bfloat16)
     for copy in sent:
         copy.wait_send()
+
+    def left(src, s_sem, r_sem):
+        pltpu.make_async_remote_copy(
+            src_ref=src, dst_ref=src, send_sem=s_sem, recv_sem=r_sem, device_id=(sp, other), device_id_type=MESH
+        ).wait_send()
+
+    for way in (0, 1):
+        for step in range(SPLIT - 1):
+            source, there = present(way, step)
+
+            @pl.when(there)
+            def _():
+                left(nb.at[source, core], np_s.at[source], np_r.at[source])
+
+        for step in range(SPLIT - 1):
+            source = part + ahead[way][2] * step
+
+            @pl.when(ahead[way][0] & (source >= 0) & (source < SPLIT))
+            def _():
+                left(nb.at[source, core], nz_s.at[way, step], nz_r.at[way, step])
+
+    for place in range(SPLIT - 1):
+        target = order[place]
+        way = 1 - (target > part).astype(jnp.int32)
+        left(ds2.at[target], fz_s.at[way, target], fz_r.at[way, target])
 
 
 def run_layer(kv, q, gate_up, down, out_weight, resid, gain, ranks, head_dim):
@@ -418,6 +496,7 @@
     dma = pltpu.SemaphoreType.DMA
     per_part = [dma((SPLIT,))] * 2
     per_near = [dma((SPLIT, 4))] * 2
+    per_way = [dma((2, SPLIT))] * 2
     anywhere = pl.BlockSpec(memory_space=pl.ANY)
     inside = pl.BlockSpec(memory_space=pltpu.VMEM)
     return pl.pallas_call(
@@ -439,12 +518,13 @@
             pltpu.VMEM((SPLIT, 2, share, model), half),
             pltpu.VMEM((SPLIT, share, model), half),
             pltpu.VMEM((SPLIT, share, model), half),
-            pltpu.VMEM((SPLIT, share, model), half),
+            pltpu.VMEM((2, SPLIT, share, model), half),
+            pltpu.VMEM((share, model), jnp.float32),
             dma((4,)),
         ]
         + per_part + per_near + per_part * 3
         + per_near * 4
-        + per_part + [dma, dma] + per_part * 4,
+        + per_part + [dma, dma] + per_way + per_part * 2 + per_way,
         compiler_params=pltpu.CompilerParams(
             collective_id=0, has_side_effects=True, vmem_limit_bytes=62 * 1024 * 1024
         ),

time: 184 us -> 176 us (0.957)
  the two profiles are of different devices: /device:TPU:26 before, /device:TPU:0 now
where the time goes in v3:
time: 176 us
  Pallas kernels  158 us (90%)
  local copies, waits for them, and re-layouts  12.7 us (7%)
  other arithmetic  5.49 us (3%)
    pallas_call x1, Pallas kernels, run_layer(): pl.pallas_call(functools.partial(layer_kernel, ranks, head_dim), out_shap...  158 us
    unnamed x12, local copies, waits for them, and re-layouts  3.74 us

profile of v3, /device:TPU:0, one launch (start us, length us, event | category | flops | bytes accessed | tf_op | source)
XLA Modules:
  0.0 176.0 jit_solution(7488868871482796244)
XLA Ops:
  0.0 0.0 copy-start
  0.0 0.0 copy-start.2
  0.0 1.1 bitcast_bitcast_fusion
  1.1 1.1 reshape.184
  2.1 0.3 multiply_reduce_fusion.1
  2.4 0.1 copy.36
  2.5 1.1 fusion
  3.7 0.8 multiply_cosine_fusion.1
  4.4 0.0 copy-start.3
  4.4 0.4 subtract_convert_fusion.3
  4.8 0.3 maximum_bitcast_fusion
  5.1 0.8 pad_maximum_fusion.kv_ref
  5.9 0.0 copy-done.2
  5.9 0.1 convert_bitcast_fusion
  6.0 0.1 copy.48
  6.1 0.3 multiply_reduce_fusion
  6.4 0.1 copy.39
  6.5 0.1 copy.40
  6.6 0.0 copy-done.3
  6.6 0.3 multiply_multiply_fusion
  6.9 0.0 copy-start.1
  6.9 0.7 subtract_convert_fusion.1
  7.6 0.5 pad_maximum_fusion.1
  8.1 0.3 convert_element_type.40
  8.4 0.8 copy.52
  9.2 0.0 copy-done.1
  9.2 0.3 copy.42
  9.5 0.3 copy.43
  9.8 0.9 slice.68
  10.7 1.5 copy.44
  12.2 0.3 copy.45
  12.5 0.1 slice.69
  12.6 3.2 %concatenate.18.gu_ref = bf16[4,128,1408]{2,1,0:T(8,128)(2,1)} concatenate(bf16[4,128,640]{2,1,0:T(8,128)(2,1)} %slice.68, bf16[4,128,640]{2,1,0:T(8,128)(2,1)S(1)} %slice.69, bf16[4,128,64]{2,1,0:T(8,128)(2,1)S(1)} %slice.70, bf16[4,128,64]{2,1,0:T(8,128)(2,1)S(1)} %slice.71), dimensions={2} | concatenate | bytes 2883584 | tf_op jit(solution)/shard_map/concatenate | solution.py:581
  15.8 0.0 copy-done
  15.8 0.8 constant_dynamic-slice_fusion.resid_ref
  16.6 157.6 %shard_map.109 = bf16[96,2048]{1,0:T(8,128)(2,1)} custom-call(bf16[4,192,256]{2,1,0:T(8,128)(2,1)} %pad_maximum_fusion.kv_ref, bf16[4,192,256]{2,1,0:T(8,128)(2,1)} %bitcast.36, bf16[4,128,1408]{2,1,0:T(8,128)(2,1)} %concatenate.18.gu_ref, bf16[4,704,128]{2,1,0:T(8,128)(2,1)} %bitcast.37, bf16[1024,2048]{1,0:T(8,128)(2,1)} %ow_ref.1, ...), custom_call_target="tpu_custom_call" | custom-call | tf_op jit(solution)/shard_map/pallas_call | solution.py:502
  174.2 1.8 %copy.54 = bf16[96,2048]{1,0:T(8,128)(2,1)} copy(bf16[96,2048]{1,0:T(8,128)(2,1)} %shard_map.109) | data formatting | bytes 786432
  (6 shorter events, 0.1 us)
Async XLA Ops:
  0.0 15.8 %copy-start = (bf16[192,2048]{1,0:T(8,128)(2,1)S(1)}, bf16[192,2048]{1,0:T(8,128)(2,1)}, u32[]{:S(2)}) copy-start(bf16[192,2048]{1,0:T(8,128)(2,1)} %param.11) | copy-start | bytes 2359300
  0.0 5.9 %copy-start.2 = (bf16[192,1024]{1,0:T(8,128)(2,1)S(1)}, bf16[192,1024]{1,0:T(8,128)(2,1)}, u32[]{:S(2)}) copy-start(bf16[192,1024]{1,0:T(8,128)(2,1)} %param.12) | copy-start | bytes 1179652
  4.4 2.2 %copy-start.3 = (f32[128]{0:T(128)S(1)}, f32[128]{0:T(128)}, u32[]{:S(2)}) copy-start(f32[128]{0:T(128)} %param.15) | copy-start | bytes 1540
  6.9 2.3 %copy-start.1 = (bf16[128,2816]{1,0:T(8,128)(2,1)S(1)}, bf16[128,2816]{1,0:T(8,128)(2,1)}, u32[]{:S(2)}) copy-start(bf16[128,2816]{1,0:T(8,128)(2,1)} %param.19) | copy-start | bytes 2162692

commit v4 on v3

--- a/solution.py
+++ b/solution.py
@@ -3,6 +3,7 @@
 
 import jax
 import jax.numpy as jnp
+import numpy as np
 from jax import lax
 from jax.experimental import pallas as pl
 from jax.experimental.pallas import tpu as pltpu
@@ -158,10 +159,15 @@
 def layer_kernel(
     ranks,
     head_dim,
-    kv_ref,
-    q_ref,
-    gu_ref,
-    dn_ref,
+    key_ref,
+    value_ref,
+    query_ref,
+    k_gain_ref,
+    q_gain_ref,
+    freq_ref,
+    gate_ref,
+    up_ref,
+    down_ref,
     ow_ref,
     resid_ref,
     gain_ref,
@@ -181,6 +187,9 @@
     ds2,
     dzb,
     acc,
+    kv_ref,
+    q_ref,
+    gu_ref,
     local_sem,
     kvz_s, kvz_r, kvx_s, kvx_r, q_s, q_r, gz_s, gz_r, dz_s, dz_r,
     gx_s, gx_r, dx_s, dx_r, gh_s, gh_r, dh_s, dh_r,
@@ -193,8 +202,8 @@
     rows = q_ref.shape[1]
     share = rows // 2
     depth = gu_ref.shape[1]
-    width = dn_ref.shape[1]
-    cols = dn_ref.shape[2]
+    width = down_ref.shape[0] // SPLIT
+    cols = down_ref.shape[1]
     group = q_ref.shape[2] // head_dim
     other = 1 - core
     flips = (1, 2, 3)
@@ -214,6 +223,54 @@
 
     def near(e):
         return part * ranks + flip(e)
+
+    def dn_own(index):
+        return down_ref.at[pl.ds(pl.multiple_of(index * width, 16), width)]
+
+    barrier = pltpu.get_barrier_semaphore()
+    for dz in range(1, SPLIT):
+        pl.semaphore_signal(barrier, inc=1, device_id=(peer_part(dz), core), device_id_type=MESH)
+    for e in flips:
+        pl.semaphore_signal(barrier, inc=1, device_id=(near(e), core), device_id_type=MESH)
+    pl.semaphore_signal(barrier, inc=1, device_id=(sp, other), device_id_type=MESH)
+
+    lane = lax.broadcasted_iota(jnp.int32, (rows, head_dim), 1)
+    spot = sp * rows + lax.broadcasted_iota(jnp.int32, (rows, head_dim), 0)
+    grid_bits = GRID_W.bit_length() - 1
+    coords = jnp.where(lane < head_dim // 2, spot >> grid_bits, spot & (GRID_W - 1))
+    angles = coords.astype(jnp.float32) * freq_ref[...]
+    first_half = (lane & (head_dim // 2 - 1)) < head_dim // 4
+    cosine = jnp.cos(angles)
+    sine = jnp.where(first_half, -jnp.sin(angles), jnp.sin(angles))
+
+    def turn(ref, head, gain):
+        x = ref[:, head * head_dim : (head + 1) * head_dim].astype(jnp.float32)
+        x = x * lax.rsqrt(jnp.mean(x * x, axis=-1, keepdims=True) + EPSILON) * gain[...]
+        quarter = head_dim // 4
+        mate = jnp.where(first_half, pltpu.roll(x, head_dim - quarter, 1), pltpu.roll(x, quarter, 1))
+        return (x * cosine + mate * sine).astype(jnp.bfloat16)
+
+    for index in range(SPLIT):
+        kv_ref[index, :, 0:head_dim] = turn(key_ref, index, k_gain_ref)
+        kv_ref[index, :, head_dim : 2 * head_dim] = value_ref[:, index * head_dim : (index + 1) * head_dim]
+    for index in range(SPLIT):
+        for head in range(group):
+            lanes = slice(head * head_dim, (head + 1) * head_dim)
+            q_ref[index, :, lanes] = turn(query_ref, index * group + head, q_gain_ref)
+    whole_lanes = width // 128 * 128
+    for index in range(SPLIT):
+        start = index * width // 128 * 128
+        skew = index * width - start
+        rests = []
+        for which, ref in enumerate((gate_ref, up_ref)):
+            block = ref[:, start : start + whole_lanes + 128]
+            if skew:
+                block = pltpu.roll(block.astype(jnp.float32), whole_lanes + 128 - skew, 1).astype(jnp.bfloat16)
+            gu_ref[index, :, which * whole_lanes : (which + 1) * whole_lanes] = block[:, :whole_lanes]
+            rests.append(block[:, whole_lanes:].astype(jnp.float32))
+        spread = lax.broadcasted_iota(jnp.int32, rests[0].shape, 1)
+        last = jnp.where(spread < width - whole_lanes, rests[0], pltpu.roll(rests[1], width - whole_lanes, 1))
+        gu_ref[index, :, 2 * whole_lanes :] = last.astype(jnp.bfloat16)
 
     sent = []
 
@@ -241,19 +298,13 @@
         pltpu.make_async_copy(kv_ref.at[part], kvb.at[part, rank], local_sem.at[0]),
         pltpu.make_async_copy(q_ref.at[part], qb.at[part], local_sem.at[1]),
         pltpu.make_async_copy(gu_ref.at[part], gu_at(sp), local_sem.at[2]),
-        pltpu.make_async_copy(dn_ref.at[part], dn_at(sp), local_sem.at[3]),
+        pltpu.make_async_copy(dn_own(part), dn_at(sp), local_sem.at[3]),
     ]
     for copy in locals_:
         copy.start()
     pad = wdn.shape[0] - width
     wdn[pl.ds(width, pad), :] = jnp.zeros((pad, wdn.shape[1]), wdn.dtype)
 
-    barrier = pltpu.get_barrier_semaphore()
-    for dz in range(1, SPLIT):
-        pl.semaphore_signal(barrier, inc=1, device_id=(peer_part(dz), core), device_id_type=MESH)
-    for e in flips:
-        pl.semaphore_signal(barrier, inc=1, device_id=(near(e), core), device_id_type=MESH)
-    pl.semaphore_signal(barrier, inc=1, device_id=(sp, other), device_id_type=MESH)
     pl.semaphore_wait(barrier, SPLIT - 1 + 3 + 1)
 
     def to_part(dz):
@@ -266,10 +317,10 @@
     for dz in range(1, SPLIT):
         send(q_ref.at[to_part(dz)], qb.at[part], q_s.at[dz], q_r.at[dz], (peer_part(dz), core))
     for e in (1, 2):
-        send(dn_ref.at[part], dn_at(sp), dx_s.at[0, e], dx_r.at[0, e], (near(e), core))
+        send(dn_own(part), dn_at(sp), dx_s.at[0, e], dx_r.at[0, e], (near(e), core))
     for dz in range(1, SPLIT):
         send(gu_ref.at[to_part(dz)], gu_at(sp), gz_s.at[dz], gz_r.at[dz], (peer_part(dz), core))
-        send(dn_ref.at[to_part(dz)], dn_at(sp), dz_s.at[dz], dz_r.at[dz], (peer_part(dz), core))
+        send(dn_own(to_part(dz)), dn_at(sp), dz_s.at[dz], dz_r.at[dz], (peer_part(dz), core))
     for dz in range(1, SPLIT):
         slot = kvb.at[from_part(dz), rank]
         landed(slot, kvz_s.at[dz], kvz_r.at[dz])
@@ -342,7 +393,7 @@
     pass_on(2)
     landed(prv, pj_s, pj_r)
     proj = pj[core].astype(jnp.float32) + prv[...].astype(jnp.float32)
-    stream = (resid_ref[...].astype(jnp.float32) + proj).astype(jnp.bfloat16)
+    stream = (resid_ref[pl.ds(pl.multiple_of(core * share, 16), share)].astype(jnp.float32) + proj).astype(jnp.bfloat16)
     st[...] = stream
     wide = stream.astype(jnp.float32)
     level = lax.rsqrt(jnp.mean(wide * wide, axis=-1, keepdims=True) + EPSILON)
@@ -486,12 +537,17 @@
         left(ds2.at[target], fz_s.at[way, target], fz_r.at[way, target])
 
 
-def run_layer(kv, q, gate_up, down, out_weight, resid, gain, ranks, head_dim):
-    rows = q.shape[1]
+def run_layer(key, value, query, k_gain, q_gain, gate, up, down, out_weight, resid, gain, ranks):
+    rows = query.shape[0]
     share = rows // 2
     model = resid.shape[1]
-    width = down.shape[1]
+    width = down.shape[0] // SPLIT
+    depth = gate.shape[0]
+    head_dim = q_gain.shape[0]
     n_sp = ranks * SPLIT
+    quarter = head_dim // 4
+    steps = np.tile(np.arange(quarter, dtype=np.float32), 4)
+    freq = jnp.asarray((np.float64(10000.0) ** (-steps / quarter)).astype(np.float32))[None, :]
     half = jnp.bfloat16
     dma = pltpu.SemaphoreType.DMA
     per_part = [dma((SPLIT,))] * 2
@@ -499,17 +555,19 @@
     per_way = [dma((2, SPLIT))] * 2
     anywhere = pl.BlockSpec(memory_space=pl.ANY)
     inside = pl.BlockSpec(memory_space=pltpu.VMEM)
+    kv_shape = (SPLIT, rows, 2 * head_dim)
+    q_shape = (SPLIT, rows, query.shape[1] // SPLIT)
     return pl.pallas_call(
         functools.partial(layer_kernel, ranks, head_dim),
         out_shape=jax.ShapeDtypeStruct((share, model), half),
-        in_specs=[anywhere] * 4 + [inside] * 3,
+        in_specs=[inside] * 8 + [anywhere] + [inside] * 3,
         out_specs=inside,
         scratch_shapes=[
-            pltpu.VMEM((SPLIT, ranks, rows, kv.shape[2]), half),
-            pltpu.VMEM(q.shape, half),
-            pltpu.VMEM(q.shape, half),
-            pltpu.VMEM(q.shape, half),
-            pltpu.VMEM((n_sp * gate_up.shape[1], gate_up.shape[2]), half),
+            pltpu.VMEM((SPLIT, ranks, rows, 2 * head_dim), half),
+            pltpu.VMEM(q_shape, half),
+            pltpu.VMEM(q_shape, half),
+            pltpu.VMEM(q_shape, half),
+            pltpu.VMEM((n_sp * depth, 2 * width), half),
             pltpu.VMEM((-(-width // 128) * 128, model), half),
             pltpu.VMEM((2, share, model), half),
             pltpu.VMEM((share, model), half),
@@ -520,6 +578,9 @@
             pltpu.VMEM((SPLIT, share, model), half),
             pltpu.VMEM((2, SPLIT, share, model), half),
             pltpu.VMEM((share, model), jnp.float32),
+            pltpu.VMEM(kv_shape, half),
+            pltpu.VMEM(q_shape, half),
+            pltpu.VMEM((SPLIT, depth, 2 * width), half),
             dma((4,)),
         ]
         + per_part + per_near + per_part * 3
@@ -528,7 +589,9 @@
         compiler_params=pltpu.CompilerParams(
             collective_id=0, has_side_effects=True, vmem_limit_bytes=62 * 1024 * 1024
         ),
-    )(kv, q, gate_up, down, out_weight, resid, gain)
+    )(
+        key, value, query, k_gain[None, :], q_gain[None, :], freq, gate, up, down, out_weight, resid, gain[None, :]
+    )
 
 
 def in_kernel(n_sp, n_tp, kv_here, head_dim, width):
@@ -557,6 +620,12 @@
         return whole_body(
             resid, query, key, value, q_gain, k_gain, out_weight, norm_gain, gate_weight, up_weight, down_weight
         )
+    hidden_part = gate_weight.shape[1] // SPLIT
+    ranks = n_sp // SPLIT
+    if in_kernel(n_sp, lax.axis_size("tp"), kv_here, head_dim, hidden_part):
+        return run_layer(
+            key, value, query, k_gain, q_gain, gate_weight, up_weight, down_weight, out_weight, resid, norm_gain, ranks
+        )
     tok_groups, hid_groups = groups_of(n_sp)
     ranks = n_sp // SPLIT
     group_size = heads_here // kv_here
@@ -573,27 +642,6 @@
     k_rot = prepare(key.reshape(rows, kv_here, head_dim), k_gain, positions)
     cut = lambda a: a.reshape(a.shape[0], SPLIT, -1).transpose(1, 0, 2).reshape(SPLIT * a.shape[0], -1)
     k_rot, val = cut(k_rot), cut(value)
-    hidden_part = gate_weight.shape[1] // SPLIT
-    if in_kernel(n_sp, lax.axis_size("tp"), kv_here, head_dim, hidden_part):
-        stack = lambda a: a.reshape(SPLIT, a.shape[0] // SPLIT, -1)
-        main = hidden_part // 128 * 128
-        gate_cut, up_cut = stack(cut(gate_weight)), stack(cut(up_weight))
-        gate_up = jnp.concatenate(
-            [gate_cut[..., :main], up_cut[..., :main], gate_cut[..., main:], up_cut[..., main:]], axis=-1
-        )
-        share = rows // 2
-        my_resid = lax.dynamic_slice_in_dim(resid, lax.axis_index("tp") * share, share, 0)
-        return run_layer(
-            stack(jnp.concatenate([k_rot, val], axis=1)),
-            stack(cut(q_rot)),
-            gate_up,
-            stack(down_weight),
-            out_weight,
-            my_resid,
-            norm_gain[None, :],
-            ranks,
-            head_dim,
-        )
     pair = swap(jnp.concatenate([k_rot, val], axis=1))
     pair = spread(pair, 0)
     q_mine = swap(cut(q_rot))

time: 176 us -> 161 us (0.915)
  local copies, waits for them, and re-layouts: 12.7 us -> 1.77 us
  other arithmetic: 5.49 us -> 0 us
    concatenate x1 -> x0, local copies, waits for them, and re-layouts: 3.23 us -> none  [body(): jnp.concatenate([gate_cut[..., :main], up_cut[..., :main], gate_cut[...,...]
    convert_element_type x3 -> x0, local copies, waits for them, and re-layouts: 2.1 us -> none  [the longest x1 1.05 us: prepare(): values = projected.astype(jnp.float32)]
    unnamed x12 -> x1, local copies, waits for them, and re-layouts: 3.74 us -> 1.77 us
where the time goes in v4:
time: 161 us
  Pallas kernels  159 us (99%)
  local copies, waits for them, and re-layouts  1.77 us (1%)
    pallas_call x1, Pallas kernels, run_layer(): pl.pallas_call(functools.partial(layer_kernel, ranks, head_dim), out_shap...  159 us

profile of v4, /device:TPU:0, one launch (start us, length us, event | category | flops | bytes accessed | tf_op | source)
XLA Modules:
  0.0 161.1 jit_solution(8675514288192236901)
XLA Ops:
  0.0 159.3 %shard_map.118 = bf16[96,2048]{1,0:T(8,128)(2,1)} custom-call(bf16[192,512]{1,0:T(8,128)(2,1)} %key_ref.1, bf16[192,512]{1,0:T(8,128)(2,1)} %value_ref.1, bf16[192,1024]{1,0:T(8,128)(2,1)} %query_ref.1, f32[1,128]{1,0:T(1,128)} %bitcast.4, f32[1,128]{1,0:T(1,128)} %bitcast.5, f32[1,128]{1,0:T(1,128)} %constant.3.freq_ref, bf16[128,2816]{1,0:T(8,128)(2,1)} %gate_ref.1, ...), custom_call_target="tpu_custom_call" | custom-call | tf_op jit(solution)/shard_map/pallas_call | solution.py:560
  159.3 1.8 %copy.14 = bf16[96,2048]{1,0:T(8,128)(2,1)} copy(bf16[96,2048]{1,0:T(8,128)(2,1)} %shard_map.118) | data formatting | bytes 786432
